TPU v7x, 32 devices: a whole 2x2x4 slice. The times are simulated.
32 devices in a mesh: sp: 8 (over z, x), tp: 4 (over y, core).
Axes of the slice: x: 2, y: 2, z: 4, core: 2. Of those that a mesh axis runs over, the one named last changes fastest.
Arguments:
- residual_in: bfloat16 [8192, 2048], P(('sp', 'tp')), may hold values from -6 to 6
- gate_outer: bfloat16 [8192, 1024], P('sp', 'tp'), may hold values from -6 to 6
- gate_inner: bfloat16 [8192, 1024], P('sp', 'tp'), may hold values from -6 to 6
- conv_input: bfloat16 [8192, 1024], P('sp', 'tp'), may hold values from -6 to 6
- conv_taps: bfloat16 [3, 1024], P(None, 'tp'), may hold values from -5 to 5
- norm_gain: bfloat16 [1024], P('tp'), may hold values from 0.099609375 to 1.8984375
- out_weight: bfloat16 [1024, 2048], P('tp'), may hold values from -0.1875 to 0.1875
- moe_gain: bfloat16 [2048], replicated, may hold values from 0.099609375 to 1.8984375
- expert_ids: int32 [8192, 2], P(('sp', 'tp')), may hold values from 0 to 7, all different within a row; in each aligned block of 256 rows (0 to 255, 256 to 511, ...) at most 128 rows name the same one
- group_prob: float32 [8192], P(('sp', 'tp')), may hold values from 0.3 to 1
- route_prob: float32 [8192, 2], P(('sp', 'tp')), may hold values from 0.1 to 1
- expert_gate: bfloat16 [8, 2048, 512], P('sp'), may hold values from -0.125 to 0.125
- expert_up: bfloat16 [8, 2048, 512], P('sp'), may hold values from -0.125 to 0.125
- expert_down: bfloat16 [8, 512, 2048], P('sp'), may hold values from -0.25 to 0.25
Outputs:
- layer_out: bfloat16 [8192, 2048], P(('sp', 'tp'))
Inputs may be any that keep to these rules, and one draw needn't show every extreme that they name: `expert_ids`: each row names 2 different experts. Within the rows of one device (aligned blocks of 256 rows) no expert is named more than 128 times.
All inputs are finite; a program needn't handle non-finite values.
Results may differ from a plain program's by a relative error of at most 0.0075.
Values may be sent and summed in bfloat16 or wider, within the bound.
No kernel may reach another device: no remote copies, remote signals or barrier semaphores. Data moves between devices by JAX's collectives and lax.ppermute only.
A program may use at most 64 MiB of HBM per device.

v0:
```python
import jax
import jax.numpy as jnp
from jax import lax
from jax.sharding import PartitionSpec as P

EPSILON = 1e-06


def from_behind(shard, axis, by):
    devices = lax.axis_size(axis)
    pairs = [(i, i + by) for i in range(devices) if 0 <= i + by < devices]
    return lax.ppermute(shard, axis, pairs)


def rms_norm(values, gain):
    floats = values.astype(jnp.float32)
    factor = lax.rsqrt(jnp.mean(floats * floats, axis=-1, keepdims=True) + EPSILON)
    return floats * factor * gain.astype(jnp.float32)


def body(
    residual_in,
    gate_outer,
    gate_inner,
    conv_input,
    conv_taps,
    norm_gain,
    out_weight,
    moe_gain,
    expert_ids,
    group_prob,
    route_prob,
    expert_gate,
    expert_up,
    expert_down,
):
    seq_rows, channels = conv_input.shape
    taps_count = conv_taps.shape[0]
    inner = gate_inner.astype(jnp.float32) * conv_input.astype(jnp.float32)
    earlier = from_behind(inner[seq_rows - (taps_count - 1) :], "sp", 1)
    padded = jnp.concatenate([earlier, inner], axis=0)
    tap_f = conv_taps.astype(jnp.float32)
    filtered = jnp.zeros((seq_rows, channels), jnp.float32)
    for offset in range(taps_count):
        filtered = filtered + tap_f[offset][None, :] * padded[offset : offset + seq_rows]
    mixed_out = (gate_outer.astype(jnp.float32) * filtered).astype(jnp.bfloat16)
    gathered = lax.all_to_all(mixed_out, "tp", split_axis=0, concat_axis=1, tiled=True)
    full_weight, full_gain = (
        lax.all_gather(out_weight, "tp", axis=0, tiled=True),
        lax.all_gather(norm_gain, "tp", axis=0, tiled=True),
    )
    normed = rms_norm(gathered, full_gain).astype(jnp.bfloat16)
    projected = jnp.dot(normed, full_weight, preferred_element_type=jnp.float32)
    residual = (residual_in.astype(jnp.float32) + projected).astype(jnp.bfloat16)
    routed_in = rms_norm(residual, moe_gain).astype(jnp.bfloat16)
    tok_rows, width = routed_in.shape
    top_count = expert_ids.shape[1]
    local_count = expert_gate.shape[0]
    group_count = lax.axis_size("sp")
    experts_all = local_count * group_count
    capacity = 2 * tok_rows * top_count // experts_all
    slots = tok_rows * top_count
    flat_e = expert_ids.reshape(-1)
    one_hot = (flat_e[:, None] == jnp.arange(experts_all, dtype=jnp.int32)[None, :]).astype(
        jnp.int32
    )
    slot_rank = jnp.sum((jnp.cumsum(one_hot, axis=0) - 1) * one_hot, axis=1)
    owner_dev = flat_e // local_count
    local_slot = flat_e % local_count
    position = (local_slot * group_count + owner_dev) * capacity + slot_rank
    source_slot = (
        jnp.full((experts_all * capacity,), slots, jnp.int32)
        .at[position]
        .set(jnp.arange(slots, dtype=jnp.int32))
    )
    rows_pad = jnp.concatenate([routed_in, jnp.zeros((1, width), jnp.bfloat16)], axis=0)
    outgoing = rows_pad[source_slot // top_count].reshape(local_count, group_count, capacity, width)
    arrived = lax.all_to_all(outgoing, "sp", split_axis=1, concat_axis=1, tiled=True)
    gate_act = jnp.einsum(
        "esrd,edf->esrf", arrived, expert_gate, preferred_element_type=jnp.float32
    )
    up_act = jnp.einsum("esrd,edf->esrf", arrived, expert_up, preferred_element_type=jnp.float32)
    hidden = (jax.nn.silu(gate_act) * up_act).astype(jnp.bfloat16)
    result = jnp.einsum(
        "esrf,efd->esrd", hidden, expert_down, preferred_element_type=jnp.float32
    ).astype(jnp.bfloat16)
    returned = lax.all_to_all(result, "sp", split_axis=1, concat_axis=1, tiled=True)
    slot_out = returned.reshape(-1, width)[position].reshape(tok_rows, top_count, width)
    weights = group_prob[:, None] * route_prob / jnp.sum(route_prob, axis=1, keepdims=True)
    expert_sum = jnp.sum(slot_out.astype(jnp.float32) * weights[:, :, None], axis=1)
    return (residual.astype(jnp.float32) + expert_sum).astype(jnp.bfloat16)


def solution(mesh):
    in_specs = (
        P(("sp", "tp"), None),
        P("sp", "tp"),
        P("sp", "tp"),
        P("sp", "tp"),
        P(None, "tp"),
        P("tp"),
        P("tp", None),
        P(),
        P(("sp", "tp"), None),
        P(("sp", "tp")),
        P(("sp", "tp"), None),
        P("sp", None, None),
        P("sp", None, None),
        P("sp", None, None),
    )
    out_specs = P(("sp", "tp"), None)
    return jax.shard_map(body, mesh=mesh, in_specs=in_specs, out_specs=out_specs, check_vma=False)
```

profile of v0, /device:TPU:0, one launch (start us, length us, event | category | flops | bytes accessed | tf_op | source)
XLA Modules:
  0.0 305.5 jit_solution(6382998400257712995)
XLA Ops:
  6.5 0.0 copy-start
  6.5 0.0 copy-start.4
  6.5 0.0 copy-start.6
  6.5 0.0 copy-start.10
  6.5 0.0 copy-start.7
  6.5 0.0 all-gather.3.cloned.1.call-start
  6.6 0.7 all-gather.3.cloned.1.call-update
  7.3 1.3 convert_multiply_fusion.3
  8.6 4.9 %collective-permute-start = (f32[2,256]{1,0:T(2,128)S(1)}, f32[2,256]{1,0:T(2,128)S(1)}, u32[]{:S(2)}, u32[]{:S(2)}) collective-permute-start(f32[2,256]{1,0:T(2,128)S(1)} %slice.37), channel_id=1, source_target_pairs={{0,4},{4,8},{8,12},{12,16},{16,20},{20,24},{24,28},{1,5},{5,9},{9,... | collective-permute-start | bytes 6152 | tf_op jit(solution)/shard_map/ppermute | solution.py:12
  13.5 0.0 copy-done.4
  13.5 0.1 copy.27
  13.6 0.1 eq.31
  13.8 0.1 eq.27
  13.9 1.1 reduce-window.6
  15.1 0.2 slice_reduce_fusion
  15.4 0.0 copy-done.6
  15.4 0.1 fusion.31
  15.5 0.0 copy-done.10
  15.5 5.1 %all-gather = bf16[4,1,256]{2,1,0:T(2,128)(2,1)S(1)} all-gather(bf16[1,1,256]{2,1,0:T(2,128)(2,1)S(1)} %reshape.144), channel_id=1, replica_groups=mesh['sp'=8,'tp'=4] {'tp'}, dimensions={0}, use_global_device_ids=true | all-gather | bytes 2560 | tf_op jit(solution)/shard_map/all_gather | solution.py:50
  20.6 0.0 copy-done.7
  20.6 0.1 copy.26
  20.7 0.1 mul.147
  20.8 0.0 collective-permute-done
  20.9 2.3 fusion.25
  23.1 3.5 %all-to-all-start = ((bf16[4,256,256]{2,1,0:T(8,128)(2,1)}), bf16[4,256,256]{2,1,0:T(8,128)(2,1)S(1)}, u32[]{:S(2)}, u32[]{:S(2)}) async-start(bf16[4,256,256]{2,1,0:T(8,128)(2,1)} %bitcast.57), calls=%async_computation | async-start | bytes 1048576 | tf_op jit(solution)/shard_map/all_to_all | solution.py:47
  26.6 2.4 scatter_custom_fusion
  29.1 12.3 %all-to-all-done = bf16[4,256,256]{2,1,0:T(8,128)(2,1)S(1)} async-done(((bf16[4,256,256]{2,1,0:T(8,128)(2,1)}), bf16[4,256,256]{2,1,0:T(8,128)(2,1)S(1)}, u32[]{:S(2)}, u32[]{:S(2)}) %all-to-all-start) | async-done | bytes 524320 | tf_op jit(solution)/shard_map/all_to_all | solution.py:47
  41.4 1.1 convert_bitcast_fusion.1
  42.5 2.6 copy.25
  45.1 0.2 fusion.26
  45.3 1.5 fusion.29
  46.7 5.0 %all-gather.3.cloned.1.call-done = bf16[1024,2048]{1,0:T(8,128)(2,1)} async-done(((bf16[256,2048]{1,0:T(8,128)(2,1)}), bf16[1024,2048]{1,0:T(8,128)(2,1)}) %all-gather.3.cloned.1.call-update) | async-done | bytes 4194320 | tf_op jit(solution)/shard_map/all_gather | solution.py:49
  51.8 3.9 %fusion.5 = (f32[256]{0:T(256)S(1)}, bf16[256,2048]{1,0:T(8,128)(2,1)S(1)}) fusion(bf16[256,1024]{0,1:T(8,128)(2,1)S(1)} %fusion.29, bf16[1024,2048]{1,0:T(8,128)(2,1)} %all-gather.3.cloned.1.call-done, bf16[256,2048]{1,0:T(8,128)(2,1)} %param.14), kind=kOutput, calls=%fused_computation.14 | convolution fusion | flops 1076887296 | bytes 6816768 | tf_op jit(solution)/shard_map/dot_general | solution.py:53
  55.6 0.0 copy-start.2
  55.7 1.0 copy-done.2
  56.6 0.3 fusion.7
  56.9 0.1 concatenate.7
  57.0 6.0 %gather_fusion = bf16[1024,2048]{1,0:T(8,128)(2,1)} fusion(bf16[257,2048]{1,0:T(8,128)(2,1)S(1)} %concatenate.7, s32[1024]{0:T(1024)S(1)} %fusion.34), kind=kCustom, calls=%fused_computation | custom fusion | bytes 8392704 | tf_op jit(solution)/shard_map/gather | solution.py:77
  63.0 0.0 copy-start.9
  63.0 99.2 %all_to_all.23 = bf16[1,8,128,2048]{3,2,0,1:T(8,128)(2,1)S(1)} all-to-all(bf16[1,8,128,2048]{3,2,0,1:T(8,128)(2,1)} %bitcast.56), channel_id=1, replica_groups=mesh['sp'=8,'tp'=4] {'sp'}, dimensions={1} | all-to-all | bytes 8388608 | tf_op jit(solution)/shard_map/all_to_all | solution.py:78
  162.2 0.0 copy-start.1
  162.2 2.0 copy-done.1
  164.2 0.0 copy-done.9
  164.2 3.7 %fusion.2 = f32[8,128,512]{2,1,0:T(8,128)} fusion(bf16[1,8,128,2048]{3,2,0,1:T(8,128)(2,1)S(1)} %all_to_all.23, bf16[1,2048,512]{2,1,0:T(8,128)(2,1)S(1)} %copy-done.9), kind=kOutput, calls=%fused_computation.5 | convolution fusion | flops 2147483648 | bytes 8388608 | tf_op jit(solution)/shard_map/esrd,edf->esrf/dot_general | solution.py:79
  167.9 0.0 copy-done
  167.9 10.0 %convert_bitcast_fusion = bf16[1,8,128,2048]{3,2,0,1:T(8,128)(2,1)} fusion(bf16[1,512,2048]{2,1,0:T(8,128)(2,1)S(1)} %copy-done, f32[8,128,512]{2,1,0:T(8,128)} %fusion.2, bf16[1,2048,512]{2,1,0:T(8,128)(2,1)} %param.26, bf16[1,8,128,2048]{3,2,0,1:T(8,128)(2,1)} %copy-done.1), kind=kOutput, calls=%fused_computation.8 | convolution fusion | flops 4300210176 | bytes 14680064 | tf_op jit(solution)/shard_map/esrf,efd->esrd/dot_general | solution.py:84
  177.9 0.0 copy-start.5
  177.9 0.0 copy-start.8
  177.9 4.9 %all-to-all-start.2 = ((bf16[1,8,128,2048]{3,2,0,1:T(8,128)(2,1)}), bf16[1,8,128,2048]{3,2,0,1:T(8,128)(2,1)}, u32[]{:S(2)}, u32[]{:S(2)}) async-start(bf16[1,8,128,2048]{3,2,0,1:T(8,128)(2,1)} %convert_bitcast_fusion), calls=%async_computation.2 | async-start | bytes 8388608 | tf_op jit(solution)/shard_map/all_to_all | solution.py:87
  182.8 0.0 copy-done.5
  182.8 0.0 copy-done.8
  182.8 0.1 copy.31
  183.0 92.0 %all-to-all-done.2 = bf16[1,8,128,2048]{3,2,0,1:T(8,128)(2,1)} async-done(((bf16[1,8,128,2048]{3,2,0,1:T(8,128)(2,1)}), bf16[1,8,128,2048]{3,2,0,1:T(8,128)(2,1)}, u32[]{:S(2)}, u32[]{:S(2)}) %all-to-all-start.2) | async-done | bytes 4194336 | tf_op jit(solution)/shard_map/all_to_all | solution.py:87
  275.0 8.0 %gather_fusion.1 = bf16[512,2048]{1,0:T(8,128)(2,1)} fusion(bf16[1024,2048]{1,0:T(8,128)(2,1)} %bitcast.22, s32[1024]{0:T(1024)S(1)} %pad_clamp_fusion), kind=kCustom, calls=%fused_computation.1 | custom fusion | bytes 4196352 | tf_op jit(solution)/shard_map/gather | solution.py:88
  282.9 5.4 %reshape.118 = f32[256,2,2048]{2,1,0:T(2,128)} reshape(bf16[512,2048]{1,0:T(8,128)(2,1)} %gather_fusion.1) | data formatting | bytes 6291456 | tf_op jit(solution)/shard_map/convert_element_type | solution.py:90
  288.4 0.0 copy-start.3
  288.4 9.0 %multiply_reduce_fusion = f32[256,2048]{1,0:T(8,128)S(1)} fusion(f32[256,2,2048]{2,1,0:T(2,128)} %reshape.118, f32[256,2]{1,0:T(8,128)S(1)} %copy.31), kind=kLoop, calls=%fused_computation.7 | loop fusion | flops 1572864 | bytes 6293504 | tf_op jit(solution)/shard_map/reduce_sum | solution.py:90
  297.4 0.0 copy-done.3
  297.4 1.3 fusion.8
  (17 shorter events, 0.1 us)
Async XLA Ops:
  6.5 161.4 %copy-start = (bf16[1,512,2048]{2,1,0:T(8,128)(2,1)S(1)}, bf16[1,512,2048]{2,1,0:T(8,128)(2,1)}, u32[]{:S(2)}) copy-start(bf16[1,512,2048]{2,1,0:T(8,128)(2,1)} %param.27) | copy-start | bytes 6291460
  6.5 7.0 %copy-start.4 = (s32[256,2]{0,1:T(2,128)S(1)}, s32[256,2]{0,1:T(2,128)}, u32[]{:S(2)}) copy-start(s32[256,2]{0,1:T(2,128)} %param.22) | copy-start | bytes 6148
  6.5 8.8 %copy-start.6 = (bf16[3,256]{1,0:T(4,128)(2,1)S(1)}, bf16[3,256]{1,0:T(4,128)(2,1)}, u32[]{:S(2)}) copy-start(bf16[3,256]{1,0:T(4,128)(2,1)} %param.18) | copy-start | bytes 4612
  6.5 8.9 %copy-start.10 = (bf16[256]{0:T(256)(128)(2,1)S(1)}, bf16[256]{0:T(256)(128)(2,1)}, u32[]{:S(2)}) copy-start(bf16[256]{0:T(256)(128)(2,1)} %param.19) | copy-start | bytes 1540
  6.5 14.0 %copy-start.7 = (bf16[2048]{0:T(1024)(128)(2,1)S(1)}, bf16[2048]{0:T(1024)(128)(2,1)}, u32[]{:S(2)}) copy-start(bf16[2048]{0:T(1024)(128)(2,1)} %param.21) | copy-start | bytes 12292
  6.5 45.2 %all-gather.3.cloned.1.call-start = ((), (), s32[]{:S(2)}) async-start(), calls=%async_computation.3 | async-start | bytes 5242880 | tf_op jit(solution)/shard_map/all_gather | solution.py:49
  8.6 12.2 %collective-permute-start = (f32[2,256]{1,0:T(2,128)S(1)}, f32[2,256]{1,0:T(2,128)S(1)}, u32[]{:S(2)}, u32[]{:S(2)}) collective-permute-start(f32[2,256]{1,0:T(2,128)S(1)} %slice.37), channel_id=1, source_target_pairs={{0,4},{4,8},{8,12},{12,16},{16,20},{20,24},{24,28},{1,5},{5,9},{9,... | collective-permute-start | bytes 6152 | tf_op jit(solution)/shard_map/ppermute | solution.py:12
  23.1 18.3 %all-to-all-start = ((bf16[4,256,256]{2,1,0:T(8,128)(2,1)}), bf16[4,256,256]{2,1,0:T(8,128)(2,1)S(1)}, u32[]{:S(2)}, u32[]{:S(2)}) async-start(bf16[4,256,256]{2,1,0:T(8,128)(2,1)} %bitcast.57), calls=%async_computation | async-start | bytes 1048576 | tf_op jit(solution)/shard_map/all_to_all | solution.py:47
  55.6 1.0 copy-start.2
  63.0 101.1 %copy-start.9 = (bf16[1,2048,512]{2,1,0:T(8,128)(2,1)S(1)}, bf16[1,2048,512]{2,1,0:T(8,128)(2,1)}, u32[]{:S(2)}) copy-start(bf16[1,2048,512]{2,1,0:T(8,128)(2,1)} %param.25) | copy-start | bytes 6291460
  162.2 2.0 copy-start.1
  177.9 4.9 %copy-start.5 = (f32[256,2]{0,1:T(2,128)S(1)}, f32[256,2]{0,1:T(2,128)}, u32[]{:S(2)}) copy-start(f32[256,2]{0,1:T(2,128)} %param.24) | copy-start | bytes 6148
  177.9 4.9 %copy-start.8 = (f32[256]{0:T(256)S(1)}, f32[256]{0:T(256)}, u32[]{:S(2)}) copy-start(f32[256]{0:T(256)} %param.23) | copy-start | bytes 3076
  177.9 97.1 %all-to-all-start.2 = ((bf16[1,8,128,2048]{3,2,0,1:T(8,128)(2,1)}), bf16[1,8,128,2048]{3,2,0,1:T(8,128)(2,1)}, u32[]{:S(2)}, u32[]{:S(2)}) async-start(bf16[1,8,128,2048]{3,2,0,1:T(8,128)(2,1)} %convert_bitcast_fusion), calls=%async_computation.2 | async-start | bytes 8388608 | tf_op jit(solution)/shard_map/all_to_all | solution.py:87
  288.4 9.0 %copy-start.3 = (bf16[256,2048]{1,0:T(8,128)(2,1)S(1)}, bf16[256,2048]{1,0:T(8,128)(2,1)}, u32[]{:S(2)}) copy-start(bf16[256,2048]{1,0:T(8,128)(2,1)} %copy-done.2) | copy-start | bytes 3145732
Sparse Core Ops, SparseCore 0:
  8.9 42.7 all-gather.2
where the time goes:
time: 306 us; the launch traced here: 305 us
  waiting for transfers between devices  110 us (36%)
  blocking collectives  104 us (34%)
  local copies, waits for them, and re-layouts  28.5 us (9%)
  other arithmetic  18.2 us (6%)
  matrix products  17.6 us (6%)
  between operations  13.6 us (4%)
  starting transfers between devices  13.2 us (4%)
    all_to_all x1, blocking collectives, body(): lax.all_to_all(outgoing, 'sp', split_axis=1, concat_axis=1, tiled=True)  99.2 us
    all_to_all x1, waiting for transfers between devices, body(): lax.all_to_all(result, 'sp', split_axis=1, concat_axis=1, tiled=True)  92 us
    all_to_all x1, waiting for transfers between devices, body(): lax.all_to_all(mixed_out, 'tp', split_axis=0, concat_axis=1, tiled=True)  12.3 us
    dot_general x1, matrix products, body(): jnp.einsum('esrf,efd->esrd', hidden, expert_down, preferred_element_type=...  9.96 us
    reduce_sum x1, other arithmetic, body(): jnp.sum(slot_out.astype(jnp.float32) * weights[:, :, None], axis=1)  8.96 us
    gather x1, local copies, waits for them, and re-layouts, body(): returned.reshape(-1, width)[position].reshape(tok_rows, top_count, width)  7.96 us
  transfers between devices with their start and end apart: 4, of which 3 were waited for; matrix products, arithmetic and copies ran while one was open for 4% of the time, Pallas kernels for 0%

commit v1 on v0

v1 whole, which is shorter than its diff:
```python
import functools

import jax
import jax.numpy as jnp
from jax import lax
from jax.experimental import pallas as pl
from jax.experimental.pallas import tpu as pltpu
from jax.sharding import PartitionSpec as P


EPSILON = 1e-06


def from_behind(shard, axis, by):
    devices = lax.axis_size(axis)
    pairs = [(i, i + by) for i in range(devices) if 0 <= i + by < devices]
    return lax.ppermute(shard, axis, pairs)


def swap(shard, axis, bit):
    devices = lax.axis_size(axis)
    return lax.ppermute(shard, axis, [(i, i ^ bit) for i in range(devices)])


def rms_norm(values, gain):
    floats = values.astype(jnp.float32)
    factor = lax.rsqrt(jnp.mean(floats * floats, axis=-1, keepdims=True) + EPSILON)
    return floats * factor * gain.astype(jnp.float32)


def mixer(gate_outer, gate_inner, conv_input, conv_taps):
    seq_rows, channels = conv_input.shape
    taps_count = conv_taps.shape[0]
    halo = taps_count - 1
    tail = slice(seq_rows - halo, seq_rows)
    earlier = from_behind(
        gate_inner[tail].astype(jnp.float32) * conv_input[tail].astype(jnp.float32), "sp", 1
    )
    inner = gate_inner.astype(jnp.float32) * conv_input.astype(jnp.float32)
    padded = jnp.concatenate([earlier, inner], axis=0)
    tap_f = conv_taps.astype(jnp.float32)
    filtered = jnp.zeros((seq_rows, channels), jnp.float32)
    for offset in range(taps_count):
        filtered = filtered + tap_f[offset][None, :] * padded[offset : offset + seq_rows]
    return (gate_outer.astype(jnp.float32) * filtered).astype(jnp.bfloat16)


def spread_tp(piece, hold=None):
    other = swap(piece, "tp", 2)
    near = swap(piece, "tp", 1)
    held = other if hold is None else after(other, hold)
    return [piece, near, held, swap(held, "tp", 1)]


def after(values, first):
    return lax.optimization_barrier((values, first))[0]


def call(kernel, outs, scratch, copies, flops, *operands, limit=40):
    at = jnp.stack([lax.axis_index("tp"), lax.axis_index("sp")]).astype(jnp.int32)
    in_vmem = pl.BlockSpec(memory_space=pltpu.VMEM)
    anywhere = pl.BlockSpec(memory_space=pltpu.HBM)
    moved = sum(a.size * a.dtype.itemsize for a in operands)
    return pl.pallas_call(
        kernel,
        out_shape=outs,
        in_specs=[pl.BlockSpec(memory_space=pltpu.SMEM)]
        + [anywhere] * copies
        + [in_vmem] * (len(operands) - copies),
        out_specs=[in_vmem] * len(outs),
        scratch_shapes=scratch + [pltpu.SemaphoreType.DMA((copies,))],
        compiler_params=pltpu.CompilerParams(vmem_limit_bytes=limit * 2**20),
        cost_estimate=pl.CostEstimate(flops=flops, bytes_accessed=moved, transcendentals=0),
    )(at, *operands)


def row_part(ref, index, count):
    return ref.at[pl.ds(pl.multiple_of(index * count, count), count)]


def project_kernel(at, w0, w1, w2, w3, res_in, mixed, moe_gain, residual, low, high, weight, held, sems):
    pieces = (w0, w1, w2, w3)
    deep, rows = w0.shape[0], res_in.shape[0]
    copies = [
        pltpu.make_async_copy(w, row_part(weight, at[0] ^ j, deep), sems.at[j])
        for j, w in enumerate(pieces)
    ]
    copies.append(pltpu.make_async_copy(res_in, held, sems.at[len(pieces)]))
    for copy in copies:
        copy.start()
    count, width = mixed.shape[0], mixed.shape[2]
    floats = [mixed[j, 0:rows].astype(jnp.float32) for j in range(count)]
    total = sum(jnp.sum(f * f, axis=-1, keepdims=True) for f in floats)
    factor = lax.rsqrt(total / (count * width) + EPSILON)
    normed = [
        (floats[j] * factor * mixed[j, rows : rows + 1].astype(jnp.float32)).astype(jnp.bfloat16)
        for j in range(count)
    ]
    for copy in copies:
        copy.wait()
    summed = jnp.dot(
        jnp.concatenate(normed, axis=1), weight[...], preferred_element_type=jnp.float32
    )
    new = (held[...].astype(jnp.float32) + summed).astype(jnp.bfloat16)
    residual[...] = new
    floats = new.astype(jnp.float32)
    scale = lax.rsqrt(jnp.mean(floats * floats, axis=-1, keepdims=True) + EPSILON)
    routed = (floats * scale * moe_gain[...].astype(jnp.float32)).astype(jnp.bfloat16)
    half = rows // 2
    low[...] = routed[:half]
    high[...] = routed[half:]


def project(mixed, pieces, res_in, moe_gain):
    rows, width = res_in.shape
    outs = [
        jax.ShapeDtypeStruct((rows, width), jnp.bfloat16),
        jax.ShapeDtypeStruct((rows // 2, width), jnp.bfloat16),
        jax.ShapeDtypeStruct((rows // 2, width), jnp.bfloat16),
    ]
    depth = mixed.shape[0] * mixed.shape[2]
    scratch = [pltpu.VMEM((depth, width), jnp.bfloat16), pltpu.VMEM((rows, width), jnp.bfloat16)]
    return call(
        project_kernel, outs, scratch, 5, 2 * rows * width * depth,
        *pieces, res_in, mixed, moe_gain[None],
    )


def hidden_kernel(gates, blocks, step, at, *refs):
    weights, rows = refs[: 2 * gates], refs[2 * gates : 2 * gates + blocks]
    out, gate, up, held, sems = refs[2 * gates + blocks :]
    deep = weights[0].shape[0]

    def fetch(n):
        if gates == 1:
            place = (gate, up)[n]
        else:
            place = row_part((gate, up)[n // gates], at[0] ^ (n % gates), deep)
        return pltpu.make_async_copy(weights[n], place, sems.at[n])

    loads, position = [], 0
    for n, x in enumerate(rows):
        place = held.at[position : position + x.shape[0]]
        loads.append((position, pltpu.make_async_copy(x, place, sems.at[2 * gates + n])))
        position += x.shape[0]
    fetches = [fetch(n) for n in range(2 * gates)]
    for copy in fetches[:gates]:
        copy.start()
    for begin, copy in loads:
        copy.start()
        if begin == 0:
            for other in fetches[gates:]:
                other.start()
    for begin in range(0, position, step):
        for first, copy in loads:
            if begin <= first < begin + step:
                copy.wait()
        if begin == 0:
            for copy in fetches[:gates]:
                copy.wait()
        span = slice(begin, begin + step)
        g = jnp.dot(held[span], gate[...], preferred_element_type=jnp.float32)
        if begin == 0:
            for copy in fetches[gates:]:
                copy.wait()
        u = jnp.dot(held[span], up[...], preferred_element_type=jnp.float32)
        out[span] = (g * jax.nn.sigmoid(g) * u).astype(jnp.bfloat16)


def hidden_of(blocks, gate, up):
    rows, depth = sum(b.shape[0] for b in blocks), blocks[0].shape[1]
    wide = gate[0].shape[1]
    kernel = functools.partial(hidden_kernel, len(gate), len(blocks), 2 * blocks[0].shape[0])
    scratch = [pltpu.VMEM((depth, wide), jnp.bfloat16)] * 2 + [pltpu.VMEM((rows, depth), jnp.bfloat16)]
    (out,) = call(
        kernel, [jax.ShapeDtypeStruct((rows, wide), jnp.bfloat16)], scratch,
        2 * len(gate) + len(blocks), 4 * rows * depth * wide, *gate, *up, *blocks,
    )
    return out


def route_slots(routed_in, residual, expert_ids, weights, expert_gate, expert_up, expert_down):
    tok_rows, width = routed_in.shape
    top_count = expert_ids.shape[1]
    local_count = expert_gate.shape[0]
    group_count = lax.axis_size("sp")
    experts_all = local_count * group_count
    capacity = 2 * tok_rows * top_count // experts_all
    slots = tok_rows * top_count
    flat_e = expert_ids.reshape(-1)
    one_hot = (flat_e[:, None] == jnp.arange(experts_all, dtype=jnp.int32)[None, :]).astype(
        jnp.int32
    )
    slot_rank = jnp.sum((jnp.cumsum(one_hot, axis=0) - 1) * one_hot, axis=1)
    owner_dev = flat_e // local_count
    local_slot = flat_e % local_count
    position = (local_slot * group_count + owner_dev) * capacity + slot_rank
    source_slot = (
        jnp.full((experts_all * capacity,), slots, jnp.int32)
        .at[position]
        .set(jnp.arange(slots, dtype=jnp.int32))
    )
    rows_pad = jnp.concatenate([routed_in, jnp.zeros((1, width), jnp.bfloat16)], axis=0)
    outgoing = rows_pad[source_slot // top_count].reshape(local_count, group_count, capacity, width)
    arrived = lax.all_to_all(outgoing, "sp", split_axis=1, concat_axis=1, tiled=True)
    gate_act = jnp.einsum(
        "esrd,edf->esrf", arrived, expert_gate, preferred_element_type=jnp.float32
    )
    up_act = jnp.einsum("esrd,edf->esrf", arrived, expert_up, preferred_element_type=jnp.float32)
    hidden = (jax.nn.silu(gate_act) * up_act).astype(jnp.bfloat16)
    result = jnp.einsum(
        "esrf,efd->esrd", hidden, expert_down, preferred_element_type=jnp.float32
    ).astype(jnp.bfloat16)
    returned = lax.all_to_all(result, "sp", split_axis=1, concat_axis=1, tiled=True)
    slot_out = returned.reshape(-1, width)[position].reshape(tok_rows, top_count, width)
    expert_sum = jnp.sum(slot_out.astype(jnp.float32) * weights[:, :, None], axis=1)
    return (residual.astype(jnp.float32) + expert_sum).astype(jnp.bfloat16)


def column_of(weights, index):
    lanes = lax.broadcasted_iota(jnp.int32, weights.shape, 1)
    return jnp.sum(jnp.where(lanes == index, weights[...], 0.0), axis=-1, keepdims=True)


def down_kernel(groups, column, at, near, *refs):
    pieces, refs = refs[:4], refs[4:]
    near_w, far_w, sems = refs[-3:]
    members, outs = len(groups), refs[-3 - len(groups) : -3]
    wide, extent = pieces[0].shape[1], near_w.shape[1]
    copies = [pltpu.make_async_copy(near.at[:, column : column + extent], near_w, sems.at[0])]
    for j, piece in enumerate(pieces):
        place = pl.ds(pl.multiple_of((at[0] ^ j) * wide, wide), wide)
        copies.append(pltpu.make_async_copy(piece, far_w.at[:, place], sems.at[1 + j]))
    for copy in copies:
        copy.start()
    far_index = at[1] ^ (lax.axis_size("sp") // 2)
    for n, (near_row, far_row, based) in enumerate(groups):
        weights, mine, theirs = refs[3 * n : 3 * n + 3]
        rows = weights.shape[0]
        own, other = column_of(weights, at[1]), column_of(weights, far_index)
        if n == 0:
            copies[0].wait()
        a = jnp.dot(mine[near_row : near_row + rows], near_w[...], preferred_element_type=jnp.float32)
        if n == 0:
            for copy in copies[1:]:
                copy.wait()
        b = jnp.dot(theirs[far_row : far_row + rows], far_w[...], preferred_element_type=jnp.float32)
        both = own * a.astype(jnp.bfloat16).astype(jnp.float32)
        both += other * b.astype(jnp.bfloat16).astype(jnp.float32)
        if based:
            both += refs[3 * members][:, column : column + extent].astype(jnp.float32)
        outs[n][...] = both.astype(outs[n].dtype)


def down_of(members, near, pieces, column, base=None):
    groups, operands, outs = [], [], []
    depth, extent = near.shape[0], pieces[0].shape[1] * len(pieces)
    for weights, near_h, near_row, far_h, far_row in members:
        groups.append((near_row, far_row, base is not None))
        operands += [weights, near_h, far_h]
        kind = jnp.bfloat16 if base is None else jnp.float32
        outs.append(jax.ShapeDtypeStruct((weights.shape[0], extent), kind))
    operands += [] if base is None else [base]
    flops = sum(4 * m[0].shape[0] * depth * extent for m in members)
    kernel = functools.partial(down_kernel, tuple(groups), column)
    scratch = [pltpu.VMEM((depth, extent), jnp.bfloat16)] * 2
    return call(kernel, outs, scratch, 5, flops, near, *pieces, *operands)


def quarter(array, axis, begin, extent):
    part = extent // lax.axis_size("tp")
    return lax.dynamic_slice_in_dim(array, begin + lax.axis_index("tp") * part, part, axis)


def share_square(mix, res_in, moe_gain, dense, expert_gate, expert_up, expert_down):
    far = lax.axis_size("sp") // 2
    across, along = 1, 2
    gate, up, down = expert_gate[0], expert_up[0], expert_down[0]
    depth, width = gate.shape[0], down.shape[1]
    cut = width // 2

    gate_q = swap(quarter(gate, 0, 0, depth), "sp", far)
    up_q = swap(quarter(up, 0, 0, depth), "sp", far)

    mixed, dense = mix(dense)
    others = [dense] + [swap(dense, "sp", b) for b in (across, along, across | along)]

    residual, low, high = mixed(res_in, moe_gain)
    x_high = swap(high, "sp", across)
    z_low = swap(low, "sp", along)
    x_low = swap(low, "sp", across)
    z_high = swap(high, "sp", along)

    far_gate = spread_tp(after(gate_q, low))
    lo_q = swap(quarter(down, 1, 0, cut), "sp", far)
    near = hidden_of([low, high], [gate], [up])
    x_high, z_low = after((x_high, z_low), near)
    d_high = swap(x_high, "sp", along)
    d_low = swap(z_low, "sp", across)
    up_q = after(up_q, z_low)
    hi_q = swap(quarter(down, 1, cut, cut), "sp", far)
    far_up = spread_tp(up_q)
    near_xz = hidden_of([x_low, x_high, z_low, z_high], [gate], [up])
    far_lo = spread_tp(after(lo_q, near_xz))
    near_d = hidden_of([d_low, d_high], [gate], [up])
    far_hi = spread_tp(after(hi_q, near_xz))
    tokens = [low, high, x_low, x_high, z_low, z_high, d_low, d_high]
    far_h = hidden_of(tokens, far_gate, far_up)

    rows = res_in.shape[0]
    to_x = (others[1], near_xz, 0, far_h, rows)
    to_z = (others[2], near_xz, rows, far_h, 2 * rows)
    to_d = (others[3], near_d, 0, far_h, 3 * rows)
    sums = []
    for column, pieces in ((0, far_lo), (cut, far_hi)):
        for_d, for_x, for_z = down_of([to_d, to_x, to_z], down, pieces, column)
        got_d = swap(for_d, "sp", across | along)
        got_x = swap(for_x, "sp", across)
        got_z = swap(for_z, "sp", along)
        (base,) = down_of([(others[0], near, 0, far_h, 0)], down, pieces, column, residual)
        total = base + (got_x.astype(jnp.float32) + got_z.astype(jnp.float32)) + got_d.astype(jnp.float32)
        sums.append(total.astype(jnp.bfloat16))
    return jnp.concatenate(sums, axis=1)


def body(
    residual_in,
    gate_outer,
    gate_inner,
    conv_input,
    conv_taps,
    norm_gain,
    out_weight,
    moe_gain,
    expert_ids,
    group_prob,
    route_prob,
    expert_gate,
    expert_up,
    expert_down,
):
    weights = group_prob[:, None] * route_prob / jnp.sum(route_prob, axis=1, keepdims=True)
    local_count, group_count = expert_gate.shape[0], lax.axis_size("sp")
    few = local_count * group_count <= 4 * expert_ids.shape[1]
    square = local_count == 1 and group_count % 8 == 0 and lax.axis_size("tp") == 4
    if not (few and square):
        mixed_out = mixer(gate_outer, gate_inner, conv_input, conv_taps)
        gathered = lax.all_to_all(mixed_out, "tp", split_axis=0, concat_axis=1, tiled=True)
        full_weight = lax.all_gather(out_weight, "tp", axis=0, tiled=True)
        full_gain = lax.all_gather(norm_gain, "tp", axis=0, tiled=True)
        normed = rms_norm(gathered, full_gain).astype(jnp.bfloat16)
        projected = jnp.dot(normed, full_weight, preferred_element_type=jnp.float32)
        residual = (residual_in.astype(jnp.float32) + projected).astype(jnp.bfloat16)
        routed_in = rms_norm(residual, moe_gain).astype(jnp.bfloat16)
        return route_slots(
            routed_in, residual, expert_ids, weights, expert_gate, expert_up, expert_down
        )
    lanes = jnp.arange(128, dtype=jnp.int32)[None]
    dense = sum(
        jnp.where(expert_ids[:, k : k + 1] == lanes, weights[:, k : k + 1], 0.0)
        for k in range(expert_ids.shape[1])
    )

    def mix(dense):
        mixed_out = mixer(gate_outer, gate_inner, conv_input, conv_taps)
        pieces = spread_tp(out_weight, mixed_out)
        parts = lax.axis_size("tp")
        blocks = mixed_out.reshape(parts, -1, mixed_out.shape[1])
        gain = jnp.broadcast_to(norm_gain, (parts, 16, norm_gain.shape[0]))
        blocks = jnp.concatenate([blocks, gain], axis=1)
        blocks = lax.all_to_all(blocks, "tp", split_axis=0, concat_axis=0)
        dense = after(dense, mixed_out)
        return functools.partial(project, blocks, pieces), dense

    return share_square(mix, residual_in, moe_gain, dense, expert_gate, expert_up, expert_down)


def solution(mesh):
    in_specs = (
        P(("sp", "tp"), None),
        P("sp", "tp"),
        P("sp", "tp"),
        P("sp", "tp"),
        P(None, "tp"),
        P("tp"),
        P("tp", None),
        P(),
        P(("sp", "tp"), None),
        P(("sp", "tp")),
        P(("sp", "tp"), None),
        P("sp", None, None),
        P("sp", None, None),
        P("sp", None, None),
    )
    out_specs = P(("sp", "tp"), None)
    return jax.shard_map(body, mesh=mesh, in_specs=in_specs, out_specs=out_specs, check_vma=False)
```

time: 306 us -> 204 us (0.67)
  blocking collectives: 104 us -> 0 us
  Pallas kernels: 0 us -> 34.5 us
  starting transfers between devices: 13.2 us -> 41.2 us
  matrix products: 17.6 us -> 0 us
  local copies, waits for them, and re-layouts: 28.5 us -> 12.2 us
  between operations: 13.6 us -> 0.33 us
  other arithmetic: 18.2 us -> 5.32 us
    ppermute x0 -> x34, waiting for transfers between devices: none -> 105 us  [swap(): return lax.ppermute(shard, axis, [(i, i ^ bit) for i in range(devices)])]
    all_to_all x2 -> x1, waiting for transfers between devices: 104 us -> 4.44 us  [mix(): blocks = lax.all_to_all(blocks, 'tp', split_axis=0, concat_axis=0)]
    all_to_all x1 -> x0, blocking collectives: 99.2 us -> none  [body(): lax.all_to_all(outgoing, 'sp', split_axis=1, concat_axis=1, tiled=True)]
    pallas_call x0 -> x9, Pallas kernels: none -> 34.5 us  [call(): pl.pallas_call(kernel, out_shape=outs, in_specs=[pl.BlockSpec(memory_spac...]
    ppermute x0 -> x34, starting transfers between devices: none -> 34.2 us  [swap(): return lax.ppermute(shard, axis, [(i, i ^ bit) for i in range(devices)])]
    dot_general x3 -> x0, matrix products: 17.6 us -> none  [the longest x1 9.96 us: body(): jnp.einsum('esrf,efd->esrd', hidden, expert_down, preferred_element_type=...]
    gather x2 -> x0, local copies, waits for them, and re-layouts: 14 us -> none  [the longest x1 7.96 us: body(): returned.reshape(-1, width)[position].reshape(tok_rows, top_count, width)]
    reduce_sum x3 -> x0, other arithmetic: 9.23 us -> none  [the longest x1 8.96 us: body(): jnp.sum(slot_out.astype(jnp.float32) * weights[:, :, None], axis=1)]
  transfers between devices with their start and end apart: 4 -> 36, of which waited for: 3 -> 17; matrix products, arithmetic and copies ran while one was open for 4% -> 4% of each run, Pallas kernels for 0% -> 17%
where the time goes in v1:
time: 204 us; the launch traced here: 203 us
  waiting for transfers between devices  110 us (54%)
  starting transfers between devices  41.2 us (20%)
  Pallas kernels  34.5 us (17%)
  local copies, waits for them, and re-layouts  12.2 us (6%)
  other arithmetic  5.32 us (3%)
    ppermute x34, waiting for transfers between devices, swap(): return lax.ppermute(shard, axis, [(i, i ^ bit) for i in range(devices)])  105 us
    pallas_call x9, Pallas kernels, call(): pl.pallas_call(kernel, out_shape=outs, in_specs=[pl.BlockSpec(memory_spac...  34.5 us
    ppermute x34, starting transfers between devices, swap(): return lax.ppermute(shard, axis, [(i, i ^ bit) for i in range(devices)])  34.2 us
    unnamed x32, local copies, waits for them, and re-layouts  7.53 us
    dynamic_slice x3, local copies, waits for them, and re-layouts, quarter(): lax.dynamic_slice_in_dim(array, begin + lax.axis_index('tp') * part, part...  4.6 us
    all_to_all x1, waiting for transfers between devices, mix(): blocks = lax.all_to_all(blocks, 'tp', split_axis=0, concat_axis=0)  4.44 us
  transfers between devices with their start and end apart: 36, of which 17 were waited for; matrix products, arithmetic and copies ran while one was open for 4% of the time, Pallas kernels for 17%

profile of v1, /device:TPU:0, one launch (start us, length us, event | category | flops | bytes accessed | tf_op | source)
XLA Modules:
  0.0 203.1 jit_solution(17235539559779561893)
XLA Ops:
  0.0 3.0 %collective-permute-start.2 = (bf16[256,2048]{1,0:T(8,128)(2,1)}, bf16[256,2048]{1,0:T(8,128)(2,1)}, u32[]{:S(2)}, u32[]{:S(2)}) collective-permute-start(bf16[256,2048]{1,0:T(8,128)(2,1)} %w0.1), channel_id=1, source_target_pairs={{0,2},{1,3},{2,0},{3,1},{4,6},{5,7},{6,4},{7,5},{8,10},{9,11},{10,... | collective-permute-start | bytes 3145736 | tf_op jit(solution)/shard_map/ppermute | solution.py:22
  3.0 0.7 convert_multiply_fusion.1
  3.7 3.5 %collective-permute-start.3 = (f32[2,256]{1,0:T(2,128)S(1)}, f32[2,256]{1,0:T(2,128)S(1)}, u32[]{:S(2)}, u32[]{:S(2)}) collective-permute-start(f32[2,256]{1,0:T(2,128)S(1)} %convert_multiply_fusion.1), channel_id=1, source_target_pairs={{0,4},{4,8},{8,12},{12,16},{16,20},{20,24},{24,28},{1,5},{5,9},{9,... | collective-permute-start | bytes 6152 | tf_op jit(solution)/shard_map/ppermute | solution.py:17
  7.2 1.3 convert_multiply_fusion
  8.6 0.4 fusion.5
  9.0 17.4 %collective-permute-done.2.w2 = bf16[256,2048]{1,0:T(8,128)(2,1)} collective-permute-done((bf16[256,2048]{1,0:T(8,128)(2,1)}, bf16[256,2048]{1,0:T(8,128)(2,1)}, u32[]{:S(2)}, u32[]{:S(2)}) %collective-permute-start.2) | collective-permute-done | bytes 1048608 | tf_op jit(solution)/shard_map/ppermute | solution.py:22
  26.5 0.8 pad_maximum_fusion.2
  27.3 3.5 %all-to-all-start = ((bf16[4,272,256]{2,1,0:T(8,128)(2,1)}), bf16[4,272,256]{2,1,0:T(8,128)(2,1)S(1)}, u32[]{:S(2)}, u32[]{:S(2)}) async-start(bf16[4,272,256]{2,1,0:T(8,128)(2,1)} %pad_maximum_fusion.2), calls=%async_computation | async-start | bytes 1114112 | tf_op jit(solution)/shard_map/all_to_all | solution.py:371
  30.8 1.9 dynamic-slice_bitcast_fusion.1
  32.7 2.8 %collective-permute-start.12 = (bf16[512,512]{1,0:T(8,128)(2,1)}, bf16[512,512]{1,0:T(8,128)(2,1)}, u32[]{:S(2)}, u32[]{:S(2)}) collective-permute-start(bf16[512,512]{1,0:T(8,128)(2,1)} %dynamic-slice_bitcast_fusion.1), channel_id=1, source_target_pairs={{0,16},{4,20},{8,24},{12,28},{16,0},{20,4},{24,8},{28,12},{1,17},{... | collective-permute-start | bytes 1572872 | tf_op jit(solution)/shard_map/ppermute | solution.py:22
  35.6 4.4 %all-to-all-done.mixed = bf16[4,272,256]{2,1,0:T(8,128)(2,1)S(1)} async-done(((bf16[4,272,256]{2,1,0:T(8,128)(2,1)}), bf16[4,272,256]{2,1,0:T(8,128)(2,1)S(1)}, u32[]{:S(2)}, u32[]{:S(2)}) %all-to-all-start) | async-done | bytes 557088 | tf_op jit(solution)/shard_map/all_to_all | solution.py:371
  40.1 0.8 copy-done.5
  40.9 1.1 copy-done.6
  41.9 1.2 copy-done.7
  43.1 1.2 copy-done.8
  44.4 5.1 %shard_map.136 = (bf16[256,2048]{1,0:T(8,128)(2,1)S(1)}, bf16[128,2048]{1,0:T(8,128)(2,1)}, bf16[128,2048]{1,0:T(8,128)(2,1)}) custom-call(s32[2]{0:T(128)S(1)} %pad_add_fusion.at, bf16[256,2048]{1,0:T(8,128)(2,1)S(1)} %copy-done.7, bf16[256,2048]{1,0:T(8,128)(2,1)} %collective-permute-done.1.w1, bf16[256,2048]{1,0:T(8,128)(2,1)} %collective-permute-done.2.w2, ...), custom_call_target="tpu_custom_call" | custom-call | flops 1073741824 | bytes 5804032 | tf_op jit(solution)/shard_map/pallas_call | solution.py:64
  49.5 1.8 collective-permute-start.7
  51.2 1.5 collective-permute-start.6
  52.7 1.9 dynamic-slice_bitcast_fusion
  54.6 2.6 %collective-permute-start.16 = (bf16[512,512]{1,0:T(8,128)(2,1)}, bf16[512,512]{1,0:T(8,128)(2,1)}, u32[]{:S(2)}, u32[]{:S(2)}) collective-permute-start(bf16[512,512]{1,0:T(8,128)(2,1)} %dynamic-slice_bitcast_fusion), channel_id=1, source_target_pairs={{0,16},{4,20},{8,24},{12,28},{16,0},{20,4},{24,8},{28,12},{1,17},{... | collective-permute-start | bytes 1572872 | tf_op jit(solution)/shard_map/ppermute | solution.py:22
  57.2 2.9 %collective-permute-done.12.refs_0_ = bf16[512,512]{1,0:T(8,128)(2,1)} collective-permute-done((bf16[512,512]{1,0:T(8,128)(2,1)}, bf16[512,512]{1,0:T(8,128)(2,1)}, u32[]{:S(2)}, u32[]{:S(2)}) %collective-permute-start.12) | collective-permute-done | bytes 524320 | tf_op jit(solution)/shard_map/ppermute | solution.py:22
  60.0 2.0 collective-permute-start.14
  62.0 0.9 dynamic-slice_bitcast_fusion.3
  62.9 13.9 %collective-permute-done.7.refs_4_.refs_12_ = bf16[128,2048]{1,0:T(8,128)(2,1)} collective-permute-done((bf16[128,2048]{1,0:T(8,128)(2,1)}, bf16[128,2048]{1,0:T(8,128)(2,1)}, u32[]{:S(2)}, u32[]{:S(2)}) %collective-permute-start.7) | collective-permute-done | bytes 524320 | tf_op jit(solution)/shard_map/ppermute | solution.py:22
  76.8 1.6 copy-done.1
  78.4 1.6 copy-done.3
  80.0 3.7 %shard_map.137.refs_5_ = bf16[256,512]{1,0:T(8,128)(2,1)S(1)} custom-call(s32[2]{0:T(128)S(1)} %pad_add_fusion.at, bf16[2048,512]{1,0:T(8,128)(2,1)S(1)} %bitcast.25, bf16[2048,512]{1,0:T(8,128)(2,1)S(1)} %bitcast.28, bf16[128,2048]{1,0:T(8,128)(2,1)} %get-tuple-element.23.refs_2_.refs_8_, bf16[128,2048]{1,0:T(8,128)(2,1)} %get-tuple-element.24.refs_3_.refs_9_), custom_call_target="tpu_custom_call" | custom-call | flops 1073741824 | bytes 5242880 | tf_op jit(solution)/shard_map/pallas_call | solution.py:64
  83.7 1.6 collective-permute-start.5
  85.2 8.5 %collective-permute-done.16.refs_4_ = bf16[512,512]{1,0:T(8,128)(2,1)} collective-permute-done((bf16[512,512]{1,0:T(8,128)(2,1)}, bf16[512,512]{1,0:T(8,128)(2,1)}, u32[]{:S(2)}, u32[]{:S(2)}) %collective-permute-start.16) | collective-permute-done | bytes 524320 | tf_op jit(solution)/shard_map/ppermute | solution.py:22
  93.7 0.5 collective-permute-start.8
  94.2 5.2 %collective-permute-done.refs_0_ = bf16[512,256]{1,0:T(8,128)(2,1)S(1)} collective-permute-done((bf16[512,256]{1,0:T(8,128)(2,1)}, bf16[512,256]{1,0:T(8,128)(2,1)S(1)}, u32[]{:S(2)}, u32[]{:S(2)}) %collective-permute-start) | collective-permute-done | bytes 262176 | tf_op jit(solution)/shard_map/ppermute | solution.py:22
  99.3 1.7 collective-permute-start.20
  101.0 3.7 %collective-permute-done.28.refs_0_ = bf16[512,256]{1,0:T(8,128)(2,1)} collective-permute-done((bf16[512,256]{1,0:T(8,128)(2,1)}, bf16[512,256]{1,0:T(8,128)(2,1)}, u32[]{:S(2)}, u32[]{:S(2)}) %collective-permute-start.28) | collective-permute-done | bytes 262176 | tf_op jit(solution)/shard_map/ppermute | solution.py:22
  104.7 1.6 collective-permute-start.18
  106.3 0.7 collective-permute-start.21
  107.2 8.7 %collective-permute-done.8.refs_5_.refs_13_ = bf16[128,2048]{1,0:T(8,128)(2,1)S(1)} collective-permute-done((bf16[128,2048]{1,0:T(8,128)(2,1)}, bf16[128,2048]{1,0:T(8,128)(2,1)S(1)}, u32[]{:S(2)}, u32[]{:S(2)}) %collective-permute-start.8) | collective-permute-done | bytes 524320 | tf_op jit(solution)/shard_map/ppermute | solution.py:22
  115.9 2.7 %collective-permute-done.18.refs_6_ = bf16[512,512]{1,0:T(8,128)(2,1)S(1)} collective-permute-done((bf16[512,512]{1,0:T(8,128)(2,1)}, bf16[512,512]{1,0:T(8,128)(2,1)S(1)}, u32[]{:S(2)}, u32[]{:S(2)}) %collective-permute-start.18) | collective-permute-done | bytes 524320 | tf_op jit(solution)/shard_map/ppermute | solution.py:22
  118.5 0.5 collective-permute-start.19
  119.0 4.6 %shard_map.138.refs_8_.refs_11_ = bf16[512,512]{1,0:T(8,128)(2,1)S(1)} custom-call(s32[2]{0:T(128)S(1)} %pad_add_fusion.at, bf16[2048,512]{1,0:T(8,128)(2,1)S(1)} %bitcast.26, bf16[2048,512]{1,0:T(8,128)(2,1)S(1)} %bitcast.29, bf16[128,2048]{1,0:T(8,128)(2,1)S(1)} %collective-permute-done.5.refs_2_.refs_10_, ...), custom_call_target="tpu_custom_call" | custom-call | flops 2147483648 | bytes 6291456 | tf_op jit(solution)/shard_map/pallas_call | solution.py:64
  123.7 3.3 %collective-permute-done.21.refs_15_.refs_3_ = bf16[128,2048]{1,0:T(8,128)(2,1)S(1)} collective-permute-done((bf16[128,2048]{1,0:T(8,128)(2,1)}, bf16[128,2048]{1,0:T(8,128)(2,1)S(1)}, u32[]{:S(2)}, u32[]{:S(2)}) %collective-permute-start.21) | collective-permute-done | bytes 524320 | tf_op jit(solution)/shard_map/ppermute | solution.py:22
  127.0 1.6 collective-permute-start.10
  128.8 2.4 %shard_map.141.refs_5_ = bf16[256,512]{1,0:T(8,128)(2,1)S(1)} custom-call(s32[2]{0:T(128)S(1)} %pad_add_fusion.at, bf16[2048,512]{1,0:T(8,128)(2,1)S(1)} %bitcast.27, bf16[2048,512]{1,0:T(8,128)(2,1)S(1)} %bitcast.30, bf16[128,2048]{1,0:T(8,128)(2,1)S(1)} %collective-permute-done.20.refs_14_.refs_2_, ...), custom_call_target="tpu_custom_call" | custom-call | flops 1073741824 | bytes 5242880 | tf_op jit(solution)/shard_map/pallas_call | solution.py:64
  131.2 0.7 collective-permute-start.22
  131.9 3.4 %collective-permute-done.10.refs_2_ = bf16[512,256]{1,0:T(8,128)(2,1)S(1)} collective-permute-done((bf16[512,256]{1,0:T(8,128)(2,1)S(1)}, bf16[512,256]{1,0:T(8,128)(2,1)S(1)}, u32[]{:S(2)}, u32[]{:S(2)}) %collective-permute-start.10) | collective-permute-done | bytes 262176 | tf_op jit(solution)/shard_map/ppermute | solution.py:22
  135.2 1.5 collective-permute-start.23
  136.9 0.5 collective-permute-start.11
  137.4 7.6 %shard_map.139.refs_6_.refs_9_.refs_12_ = bf16[1024,512]{1,0:T(8,128)(2,1)S(1)} custom-call(s32[2]{0:T(128)S(1)} %pad_add_fusion.at, bf16[512,512]{1,0:T(8,128)(2,1)} %collective-permute-done.12.refs_0_, bf16[512,512]{1,0:T(8,128)(2,1)S(1)} %collective-permute-done.13.refs_1_, bf16[512,512]{1,0:T(8,128)(2,1)} %collective-permute-done.14.refs_2_, ...), custom_call_target="tpu_custom_call" | custom-call | flops 4294967296 | bytes 8388608 | tf_op jit(solution)/shard_map/pallas_call | solution.py:64
  145.0 1.7 collective-permute-start.30
  146.6 3.4 %shard_map.142 = (bf16[256,1024]{1,0:T(8,128)(2,1)S(1)}, bf16[256,1024]{1,0:T(8,128)(2,1)S(1)}, bf16[256,1024]{1,0:T(8,128)(2,1)S(1)}) custom-call(s32[2]{0:T(128)S(1)} %pad_add_fusion.at, bf16[512,2048]{1,0:T(8,128)(2,1)S(1)} %bitcast.21, bf16[512,256]{1,0:T(8,128)(2,1)S(1)} %collective-permute-done.refs_0_, ...), custom_call_target="tpu_custom_call" | custom-call | flops 1610612736 | bytes 7995392 | tf_op jit(solution)/shard_map/pallas_call | solution.py:64
  150.1 0.5 collective-permute-start.25
  150.6 2.9 %collective-permute-done.30.refs_2_ = bf16[512,256]{1,0:T(8,128)(2,1)S(1)} collective-permute-done((bf16[512,256]{1,0:T(8,128)(2,1)}, bf16[512,256]{1,0:T(8,128)(2,1)S(1)}, u32[]{:S(2)}, u32[]{:S(2)}) %collective-permute-start.30) | collective-permute-done | bytes 262176 | tf_op jit(solution)/shard_map/ppermute | solution.py:22
  153.5 1.9 collective-permute-start.26
  155.5 3.4 %shard_map.144 = (bf16[256,1024]{1,0:T(8,128)(2,1)S(1)}, bf16[256,1024]{1,0:T(8,128)(2,1)S(1)}, bf16[256,1024]{1,0:T(8,128)(2,1)S(1)}) custom-call(s32[2]{0:T(128)S(1)} %pad_add_fusion.at, bf16[512,2048]{1,0:T(8,128)(2,1)S(1)} %bitcast.22, bf16[512,256]{1,0:T(8,128)(2,1)} %collective-permute-done.28.refs_0_, ...), custom_call_target="tpu_custom_call" | custom-call | flops 1610612736 | bytes 7995392 | tf_op jit(solution)/shard_map/pallas_call | solution.py:64
  158.9 1.6 collective-permute-start.32
  160.5 1.9 collective-permute-start.33
  162.5 2.4 %collective-permute-done.25 = bf16[256,1024]{1,0:T(8,128)(2,1)S(1)} collective-permute-done((bf16[256,1024]{1,0:T(8,128)(2,1)S(1)}, bf16[256,1024]{1,0:T(8,128)(2,1)S(1)}, u32[]{:S(2)}, u32[]{:S(2)}) %collective-permute-start.25) | collective-permute-done | bytes 524320 | tf_op jit(solution)/shard_map/ppermute | solution.py:22
  164.9 1.8 collective-permute-start.34
  166.8 2.1 %shard_map.140 = f32[256,1024]{1,0:T(8,128)S(1)} custom-call(s32[2]{0:T(128)S(1)} %pad_add_fusion.at, bf16[512,2048]{1,0:T(8,128)(2,1)S(1)} %bitcast.23, bf16[512,256]{1,0:T(8,128)(2,1)S(1)} %collective-permute-done.refs_0_, bf16[512,256]{1,0:T(8,128)(2,1)S(1)} %collective-permute-done.9.refs_1_, bf16[512,256]{1,0:T(8,128)(2,1)S(1)} %collective-permute-done.10.refs_2_, ...), custom_call_target="tpu_custom_call" | custom-call | flops 536870912 | bytes 5636096 | tf_op jit(solution)/shard_map/pallas_call | solution.py:64
  168.8 2.3 %shard_map.143 = f32[256,1024]{1,0:T(8,128)S(1)} custom-call(s32[2]{0:T(128)S(1)} %pad_add_fusion.at, bf16[512,2048]{1,0:T(8,128)(2,1)S(1)} %bitcast.24, bf16[512,256]{1,0:T(8,128)(2,1)} %collective-permute-done.28.refs_0_, bf16[512,256]{1,0:T(8,128)(2,1)S(1)} %collective-permute-done.29.refs_1_, bf16[512,256]{1,0:T(8,128)(2,1)S(1)} %collective-permute-done.30.refs_2_, ...), custom_call_target="tpu_custom_call" | custom-call | flops 536870912 | bytes 5636096 | tf_op jit(solution)/shard_map/pallas_call | solution.py:64
  171.1 8.4 %collective-permute-done.27 = bf16[256,1024]{1,0:T(8,128)(2,1)S(1)} collective-permute-done((bf16[256,1024]{1,0:T(8,128)(2,1)S(1)}, bf16[256,1024]{1,0:T(8,128)(2,1)S(1)}, u32[]{:S(2)}, u32[]{:S(2)}) %collective-permute-start.27) | collective-permute-done | bytes 524320 | tf_op jit(solution)/shard_map/ppermute | solution.py:22
  179.9 6.3 %collective-permute-done.32 = bf16[256,1024]{1,0:T(8,128)(2,1)S(1)} collective-permute-done((bf16[256,1024]{1,0:T(8,128)(2,1)S(1)}, bf16[256,1024]{1,0:T(8,128)(2,1)S(1)}, u32[]{:S(2)}, u32[]{:S(2)}) %collective-permute-start.32) | collective-permute-done | bytes 524320 | tf_op jit(solution)/shard_map/ppermute | solution.py:22
  186.2 4.6 %collective-permute-done.33 = bf16[256,1024]{1,0:T(8,128)(2,1)S(1)} collective-permute-done((bf16[256,1024]{1,0:T(8,128)(2,1)S(1)}, bf16[256,1024]{1,0:T(8,128)(2,1)S(1)}, u32[]{:S(2)}, u32[]{:S(2)}) %collective-permute-start.33) | collective-permute-done | bytes 524320 | tf_op jit(solution)/shard_map/ppermute | solution.py:22
  190.9 10.9 %collective-permute-done.34 = bf16[256,1024]{1,0:T(8,128)(2,1)S(1)} collective-permute-done((bf16[256,1024]{1,0:T(8,128)(2,1)S(1)}, bf16[256,1024]{1,0:T(8,128)(2,1)S(1)}, u32[]{:S(2)}, u32[]{:S(2)}) %collective-permute-start.34) | collective-permute-done | bytes 524320 | tf_op jit(solution)/shard_map/ppermute | solution.py:22
  202.1 1.1 pad_maximum_fusion.1
  (68 shorter events, 1.3 us)
Async XLA Ops:
  0.0 8.6 %copy-start.11 = (bf16[3,256]{1,0:T(4,128)(2,1)S(1)}, bf16[3,256]{1,0:T(4,128)(2,1)}, u32[]{:S(2)}) copy-start(bf16[3,256]{1,0:T(4,128)(2,1)} %param.18) | copy-start | bytes 4612
  0.0 8.6 %copy-start.9 = (bf16[1024,256]{1,0:T(8,128)(2,1)S(1)}, bf16[1024,256]{1,0:T(8,128)(2,1)}, u32[]{:S(2)}) copy-start(bf16[1024,256]{1,0:T(8,128)(2,1)} %param.15) | copy-start | bytes 1572868
  0.0 26.5 %collective-permute-start.2 = (bf16[256,2048]{1,0:T(8,128)(2,1)}, bf16[256,2048]{1,0:T(8,128)(2,1)}, u32[]{:S(2)}, u32[]{:S(2)}) collective-permute-start(bf16[256,2048]{1,0:T(8,128)(2,1)} %w0.1), channel_id=1, source_target_pairs={{0,2},{1,3},{2,0},{3,1},{4,6},{5,7},{6,4},{7,5},{8,10},{9,11},{10,... | collective-permute-start | bytes 3145736 | tf_op jit(solution)/shard_map/ppermute | solution.py:22
  3.0 37.9 %collective-permute-start.1 = (bf16[256,2048]{1,0:T(8,128)(2,1)}, bf16[256,2048]{1,0:T(8,128)(2,1)}, u32[]{:S(2)}, u32[]{:S(2)}) collective-permute-start(bf16[256,2048]{1,0:T(8,128)(2,1)} %w0.1), channel_id=1, source_target_pairs={{0,1},{1,0},{2,3},{3,2},{4,5},{5,4},{6,7},{7,6},{8,9},{9,8},{10,11... | collective-permute-start | bytes 3145736 | tf_op jit(solution)/shard_map/ppermute | solution.py:22
  3.7 22.8 %copy-start.15 = (bf16[256]{0:T(256)(128)(2,1)S(1)}, bf16[256]{0:T(256)(128)(2,1)}, u32[]{:S(2)}) copy-start(bf16[256]{0:T(256)(128)(2,1)} %param.19) | copy-start | bytes 1540
  3.7 4.9 %collective-permute-start.3 = (f32[2,256]{1,0:T(2,128)S(1)}, f32[2,256]{1,0:T(2,128)S(1)}, u32[]{:S(2)}, u32[]{:S(2)}) collective-permute-start(f32[2,256]{1,0:T(2,128)S(1)} %convert_multiply_fusion.1), channel_id=1, source_target_pairs={{0,4},{4,8},{8,12},{12,16},{16,20},{20,24},{24,28},{1,5},{5,9},{9,... | collective-permute-start | bytes 6152 | tf_op jit(solution)/shard_map/ppermute | solution.py:17
  9.0 26.6 %copy-start.12 = (bf16[2048]{0:T(1024)(128)(2,1)S(1)}, bf16[2048]{0:T(1024)(128)(2,1)}, u32[]{:S(2)}) copy-start(bf16[2048]{0:T(1024)(128)(2,1)} %param.21) | copy-start | bytes 12292
  26.5 14.4 %collective-permute-start.4 = (bf16[256,2048]{1,0:T(8,128)(2,1)}, bf16[256,2048]{1,0:T(8,128)(2,1)}, u32[]{:S(2)}, u32[]{:S(2)}) collective-permute-start(bf16[256,2048]{1,0:T(8,128)(2,1)} %collective-permute-done.2.w2), channel_id=1, source_target_pairs={{0,1},{1,0},{2,3},{3,2},{4,5},{5,4},{6,7},{7,6},{8,9},{9,8},{10,11... | collective-permute-start | bytes 3145736 | tf_op jit(solution)/shard_map/ppermute | solution.py:22
  27.3 12.7 %all-to-all-start = ((bf16[4,272,256]{2,1,0:T(8,128)(2,1)}), bf16[4,272,256]{2,1,0:T(8,128)(2,1)S(1)}, u32[]{:S(2)}, u32[]{:S(2)}) async-start(bf16[4,272,256]{2,1,0:T(8,128)(2,1)} %pad_maximum_fusion.2), calls=%async_computation | async-start | bytes 1114112 | tf_op jit(solution)/shard_map/all_to_all | solution.py:371
  32.7 27.3 %collective-permute-start.12 = (bf16[512,512]{1,0:T(8,128)(2,1)}, bf16[512,512]{1,0:T(8,128)(2,1)}, u32[]{:S(2)}, u32[]{:S(2)}) collective-permute-start(bf16[512,512]{1,0:T(8,128)(2,1)} %dynamic-slice_bitcast_fusion.1), channel_id=1, source_target_pairs={{0,16},{4,20},{8,24},{12,28},{16,0},{20,4},{24,8},{28,12},{1,17},{... | collective-permute-start | bytes 1572872 | tf_op jit(solution)/shard_map/ppermute | solution.py:22
  35.6 26.4 %copy-start = (bf16[1,512,2048]{2,1,0:T(8,128)(2,1)S(1)}, bf16[1,512,2048]{2,1,0:T(8,128)(2,1)}, u32[]{:S(2)}) copy-start(bf16[1,512,2048]{2,1,0:T(8,128)(2,1)} %param.27) | copy-start | bytes 6291460
  40.1 0.8 copy-start.5
  40.9 1.1 copy-start.6
  41.9 1.2 copy-start.7
  43.1 1.2 copy-start.8
  49.4 27.3 %copy-start.10 = (f32[256,2]{0,1:T(2,128)S(1)}, f32[256,2]{0,1:T(2,128)}, u32[]{:S(2)}) copy-start(f32[256,2]{0,1:T(2,128)} %param.24) | copy-start | bytes 6148
  49.5 27.3 %collective-permute-start.7 = (bf16[128,2048]{1,0:T(8,128)(2,1)}, bf16[128,2048]{1,0:T(8,128)(2,1)}, u32[]{:S(2)}, u32[]{:S(2)}) collective-permute-start(bf16[128,2048]{1,0:T(8,128)(2,1)} %get-tuple-element.23.refs_2_.refs_8_), channel_id=1, source_target_pairs={{0,8},{4,12},{8,0},{12,4},{16,24},{20,28},{24,16},{28,20},{1,9},{5... | collective-permute-start | bytes 1572872 | tf_op jit(solution)/shard_map/ppermute | solution.py:22
  51.2 32.5 %collective-permute-start.6 = (bf16[128,2048]{1,0:T(8,128)(2,1)}, bf16[128,2048]{1,0:T(8,128)(2,1)}, u32[]{:S(2)}, u32[]{:S(2)}) collective-permute-start(bf16[128,2048]{1,0:T(8,128)(2,1)} %get-tuple-element.24.refs_3_.refs_9_), channel_id=1, source_target_pairs={{0,4},{4,0},{8,12},{12,8},{16,20},{20,16},{24,28},{28,24},{1,5},{5... | collective-permute-start | bytes 1572872 | tf_op jit(solution)/shard_map/ppermute | solution.py:22
  54.6 39.1 %collective-permute-start.16 = (bf16[512,512]{1,0:T(8,128)(2,1)}, bf16[512,512]{1,0:T(8,128)(2,1)}, u32[]{:S(2)}, u32[]{:S(2)}) collective-permute-start(bf16[512,512]{1,0:T(8,128)(2,1)} %dynamic-slice_bitcast_fusion), channel_id=1, source_target_pairs={{0,16},{4,20},{8,24},{12,28},{16,0},{20,4},{24,8},{28,12},{1,17},{... | collective-permute-start | bytes 1572872 | tf_op jit(solution)/shard_map/ppermute | solution.py:22
  60.0 46.3 %collective-permute-start.14 = (bf16[512,512]{1,0:T(8,128)(2,1)}, bf16[512,512]{1,0:T(8,128)(2,1)}, u32[]{:S(2)}, u32[]{:S(2)}) collective-permute-start(bf16[512,512]{1,0:T(8,128)(2,1)} %collective-permute-done.12.refs_0_), channel_id=1, source_target_pairs={{0,2},{1,3},{2,0},{3,1},{4,6},{5,7},{6,4},{7,5},{8,10},{9,11},{10,... | collective-permute-start | bytes 1572872 | tf_op jit(solution)/shard_map/ppermute | solution.py:22
  62.9 36.4 %collective-permute-start = (bf16[512,256]{1,0:T(8,128)(2,1)}, bf16[512,256]{1,0:T(8,128)(2,1)S(1)}, u32[]{:S(2)}, u32[]{:S(2)}) collective-permute-start(bf16[512,256]{1,0:T(8,128)(2,1)} %get-tuple-element.39), channel_id=1, source_target_pairs={{0,16},{4,20},{8,24},{12,28},{16,0},{20,4},{24,8},{28,12},{1,17},{... | collective-permute-start | bytes 786440 | tf_op jit(solution)/shard_map/ppermute | solution.py:22
  76.7 28.0 %collective-permute-start.28 = (bf16[512,256]{1,0:T(8,128)(2,1)}, bf16[512,256]{1,0:T(8,128)(2,1)}, u32[]{:S(2)}, u32[]{:S(2)}) collective-permute-start(bf16[512,256]{1,0:T(8,128)(2,1)} %get-tuple-element.40), channel_id=1, source_target_pairs={{0,16},{4,20},{8,24},{12,28},{16,0},{20,4},{24,8},{28,12},{1,17},{... | collective-permute-start | bytes 786440 | tf_op jit(solution)/shard_map/ppermute | solution.py:22
  76.8 1.6 copy-start.1
  78.4 1.6 copy-start.3
  80.0 26.4 %copy-start.14 = (f32[256]{0:T(256)S(1)}, f32[256]{0:T(256)}, u32[]{:S(2)}) copy-start(f32[256]{0:T(256)} %param.23) | copy-start | bytes 3076
  80.0 27.1 %copy-start.13 = (s32[256,2]{0,1:T(2,128)S(1)}, s32[256,2]{0,1:T(2,128)}, u32[]{:S(2)}) copy-start(s32[256,2]{0,1:T(2,128)} %param.22) | copy-start | bytes 6148
  80.0 39.1 %copy-start.2 = (bf16[1,2048,512]{2,1,0:T(8,128)(2,1)S(1)}, bf16[1,2048,512]{2,1,0:T(8,128)(2,1)}, u32[]{:S(2)}) copy-start(bf16[1,2048,512]{2,1,0:T(8,128)(2,1)} %param.25) | copy-start | bytes 6291460
  80.0 39.1 %copy-start.4 = (bf16[1,2048,512]{2,1,0:T(8,128)(2,1)S(1)}, bf16[1,2048,512]{2,1,0:T(8,128)(2,1)}, u32[]{:S(2)}) copy-start(bf16[1,2048,512]{2,1,0:T(8,128)(2,1)} %param.26) | copy-start | bytes 6291460
  83.7 23.4 %collective-permute-start.5 = (bf16[128,2048]{1,0:T(8,128)(2,1)}, bf16[128,2048]{1,0:T(8,128)(2,1)S(1)}, u32[]{:S(2)}, u32[]{:S(2)}) collective-permute-start(bf16[128,2048]{1,0:T(8,128)(2,1)} %get-tuple-element.23.refs_2_.refs_8_), channel_id=1, source_target_pairs={{0,4},{4,0},{8,12},{12,8},{16,20},{20,16},{24,28},{28,24},{1,5},{5... | collective-permute-start | bytes 1572872 | tf_op jit(solution)/shard_map/ppermute | solution.py:22
  93.7 22.2 %collective-permute-start.8 = (bf16[128,2048]{1,0:T(8,128)(2,1)}, bf16[128,2048]{1,0:T(8,128)(2,1)S(1)}, u32[]{:S(2)}, u32[]{:S(2)}) collective-permute-start(bf16[128,2048]{1,0:T(8,128)(2,1)} %get-tuple-element.24.refs_3_.refs_9_), channel_id=1, source_target_pairs={{0,8},{4,12},{8,0},{12,4},{16,24},{20,28},{24,16},{28,20},{1,9},{5... | collective-permute-start | bytes 1572872 | tf_op jit(solution)/shard_map/ppermute | solution.py:22
  99.3 19.2 %collective-permute-start.20 = (bf16[128,2048]{1,0:T(8,128)(2,1)}, bf16[128,2048]{1,0:T(8,128)(2,1)S(1)}, u32[]{:S(2)}, u32[]{:S(2)}) collective-permute-start(bf16[128,2048]{1,0:T(8,128)(2,1)} %collective-permute-done.7.refs_4_.refs_12_), channel_id=1, source_target_pairs={{0,4},{4,0},{8,12},{12,8},{16,20},{20,16},{24,28},{28,24},{1,5},{5... | collective-permute-start | bytes 1572872 | tf_op jit(solution)/shard_map/ppermute | solution.py:22
  104.7 13.8 %collective-permute-start.18 = (bf16[512,512]{1,0:T(8,128)(2,1)}, bf16[512,512]{1,0:T(8,128)(2,1)S(1)}, u32[]{:S(2)}, u32[]{:S(2)}) collective-permute-start(bf16[512,512]{1,0:T(8,128)(2,1)} %collective-permute-done.16.refs_4_), channel_id=1, source_target_pairs={{0,2},{1,3},{2,0},{3,1},{4,6},{5,7},{6,4},{7,5},{8,10},{9,11},{10,... | collective-permute-start | bytes 1572872 | tf_op jit(solution)/shard_map/ppermute | solution.py:22
  106.3 20.6 %collective-permute-start.21 = (bf16[128,2048]{1,0:T(8,128)(2,1)}, bf16[128,2048]{1,0:T(8,128)(2,1)S(1)}, u32[]{:S(2)}, u32[]{:S(2)}) collective-permute-start(bf16[128,2048]{1,0:T(8,128)(2,1)} %collective-permute-done.6.refs_3_.refs_11_), channel_id=1, source_target_pairs={{0,8},{4,12},{8,0},{12,4},{16,24},{20,28},{24,16},{28,20},{1,9},{5... | collective-permute-start | bytes 1572872 | tf_op jit(solution)/shard_map/ppermute | solution.py:22
  107.1 24.1 %collective-permute-start.13 = (bf16[512,512]{1,0:T(8,128)(2,1)}, bf16[512,512]{1,0:T(8,128)(2,1)S(1)}, u32[]{:S(2)}, u32[]{:S(2)}) collective-permute-start(bf16[512,512]{1,0:T(8,128)(2,1)} %collective-permute-done.12.refs_0_), channel_id=1, source_target_pairs={{0,1},{1,0},{2,3},{3,2},{4,5},{5,4},{6,7},{7,6},{8,9},{9,8},{10,11... | collective-permute-start | bytes 1572872 | tf_op jit(solution)/shard_map/ppermute | solution.py:22
  115.8 20.9 %collective-permute-start.17 = (bf16[512,512]{1,0:T(8,128)(2,1)}, bf16[512,512]{1,0:T(8,128)(2,1)S(1)}, u32[]{:S(2)}, u32[]{:S(2)}) collective-permute-start(bf16[512,512]{1,0:T(8,128)(2,1)} %collective-permute-done.16.refs_4_), channel_id=1, source_target_pairs={{0,1},{1,0},{2,3},{3,2},{4,5},{5,4},{6,7},{7,6},{8,9},{9,8},{10,11... | collective-permute-start | bytes 1572872 | tf_op jit(solution)/shard_map/ppermute | solution.py:22
  118.5 18.3 %collective-permute-start.15 = (bf16[512,512]{1,0:T(8,128)(2,1)}, bf16[512,512]{1,0:T(8,128)(2,1)S(1)}, u32[]{:S(2)}, u32[]{:S(2)}) collective-permute-start(bf16[512,512]{1,0:T(8,128)(2,1)} %collective-permute-done.14.refs_2_), channel_id=1, source_target_pairs={{0,1},{1,0},{2,3},{3,2},{4,5},{5,4},{6,7},{7,6},{8,9},{9,8},{10,11... | collective-permute-start | bytes 1572872 | tf_op jit(solution)/shard_map/ppermute | solution.py:22
  118.5 18.3 %collective-permute-start.19 = (bf16[512,512]{1,0:T(8,128)(2,1)S(1)}, bf16[512,512]{1,0:T(8,128)(2,1)S(1)}, u32[]{:S(2)}, u32[]{:S(2)}) collective-permute-start(bf16[512,512]{1,0:T(8,128)(2,1)S(1)} %collective-permute-done.18.refs_6_), channel_id=1, source_target_pairs={{0,1},{1,0},{2,3},{3,2},{4,5},{5,4},{6,7},{7,6},{8,9},{9,8},{10,11... | collective-permute-start | bytes 1572872 | tf_op jit(solution)/shard_map/ppermute | solution.py:22
  127.0 8.2 %collective-permute-start.10 = (bf16[512,256]{1,0:T(8,128)(2,1)S(1)}, bf16[512,256]{1,0:T(8,128)(2,1)S(1)}, u32[]{:S(2)}, u32[]{:S(2)}) collective-permute-start(bf16[512,256]{1,0:T(8,128)(2,1)S(1)} %collective-permute-done.refs_0_), channel_id=1, source_target_pairs={{0,2},{1,3},{2,0},{3,1},{4,6},{5,7},{6,4},{7,5},{8,10},{9,11},{10,... | collective-permute-start | bytes 786440 | tf_op jit(solution)/shard_map/ppermute | solution.py:22
  131.2 13.8 %collective-permute-start.22 = (f32[256,128]{1,0:T(8,128)S(1)}, f32[256,128]{1,0:T(8,128)S(1)}, u32[]{:S(2)}, u32[]{:S(2)}) collective-permute-start(f32[256,128]{1,0:T(8,128)S(1)} %select_add_fusion.refs_4_), channel_id=1, source_target_pairs={{0,12},{4,8},{8,4},{12,0},{16,28},{20,24},{24,20},{28,16},{1,13},{... | collective-permute-start | bytes 393224 | tf_op jit(solution)/shard_map/ppermute | solution.py:22
  135.2 11.4 %collective-permute-start.23 = (f32[256,128]{1,0:T(8,128)S(1)}, f32[256,128]{1,0:T(8,128)S(1)}, u32[]{:S(2)}, u32[]{:S(2)}) collective-permute-start(f32[256,128]{1,0:T(8,128)S(1)} %select_add_fusion.refs_4_), channel_id=1, source_target_pairs={{0,4},{4,0},{8,12},{12,8},{16,20},{20,16},{24,28},{28,24},{1,5},{5... | collective-permute-start | bytes 393224 | tf_op jit(solution)/shard_map/ppermute | solution.py:22
  136.8 9.9 %collective-permute-start.24 = (f32[256,128]{1,0:T(8,128)S(1)}, f32[256,128]{1,0:T(8,128)S(1)}, u32[]{:S(2)}, u32[]{:S(2)}) collective-permute-start(f32[256,128]{1,0:T(8,128)S(1)} %select_add_fusion.refs_4_), channel_id=1, source_target_pairs={{0,8},{4,12},{8,0},{12,4},{16,24},{20,28},{24,16},{28,20},{1,9},{5... | collective-permute-start | bytes 393224 | tf_op jit(solution)/shard_map/ppermute | solution.py:22
  136.8 9.9 %collective-permute-start.9 = (bf16[512,256]{1,0:T(8,128)(2,1)S(1)}, bf16[512,256]{1,0:T(8,128)(2,1)S(1)}, u32[]{:S(2)}, u32[]{:S(2)}) collective-permute-start(bf16[512,256]{1,0:T(8,128)(2,1)S(1)} %collective-permute-done.refs_0_), channel_id=1, source_target_pairs={{0,1},{1,0},{2,3},{3,2},{4,5},{5,4},{6,7},{7,6},{8,9},{9,8},{10,11... | collective-permute-start | bytes 786440 | tf_op jit(solution)/shard_map/ppermute | solution.py:22
  136.9 9.8 %collective-permute-start.11 = (bf16[512,256]{1,0:T(8,128)(2,1)S(1)}, bf16[512,256]{1,0:T(8,128)(2,1)S(1)}, u32[]{:S(2)}, u32[]{:S(2)}) collective-permute-start(bf16[512,256]{1,0:T(8,128)(2,1)S(1)} %collective-permute-done.10.refs_2_), channel_id=1, source_target_pairs={{0,1},{1,0},{2,3},{3,2},{4,5},{5,4},{6,7},{7,6},{8,9},{9,8},{10,11... | collective-permute-start | bytes 786440 | tf_op jit(solution)/shard_map/ppermute | solution.py:22
  145.0 8.6 %collective-permute-start.30 = (bf16[512,256]{1,0:T(8,128)(2,1)}, bf16[512,256]{1,0:T(8,128)(2,1)S(1)}, u32[]{:S(2)}, u32[]{:S(2)}) collective-permute-start(bf16[512,256]{1,0:T(8,128)(2,1)} %collective-permute-done.28.refs_0_), channel_id=1, source_target_pairs={{0,2},{1,3},{2,0},{3,1},{4,6},{5,7},{6,4},{7,5},{8,10},{9,11},{10,... | collective-permute-start | bytes 786440 | tf_op jit(solution)/shard_map/ppermute | solution.py:22
  150.1 14.9 %collective-permute-start.25 = (bf16[256,1024]{1,0:T(8,128)(2,1)S(1)}, bf16[256,1024]{1,0:T(8,128)(2,1)S(1)}, u32[]{:S(2)}, u32[]{:S(2)}) collective-permute-start(bf16[256,1024]{1,0:T(8,128)(2,1)S(1)} %get-tuple-element.32), channel_id=1, source_target_pairs={{0,4},{4,0},{8,12},{12,8},{16,20},{20,16},{24,28},{28,24},{1,5},{5... | collective-permute-start | bytes 1572872 | tf_op jit(solution)/shard_map/ppermute | solution.py:22
  150.6 4.9 %collective-permute-start.29 = (bf16[512,256]{1,0:T(8,128)(2,1)}, bf16[512,256]{1,0:T(8,128)(2,1)S(1)}, u32[]{:S(2)}, u32[]{:S(2)}) collective-permute-start(bf16[512,256]{1,0:T(8,128)(2,1)} %collective-permute-done.28.refs_0_), channel_id=1, source_target_pairs={{0,1},{1,0},{2,3},{3,2},{4,5},{5,4},{6,7},{7,6},{8,9},{9,8},{10,11... | collective-permute-start | bytes 786440 | tf_op jit(solution)/shard_map/ppermute | solution.py:22
  153.5 2.0 collective-permute-start.31
  153.5 17.6 %collective-permute-start.26 = (bf16[256,1024]{1,0:T(8,128)(2,1)S(1)}, bf16[256,1024]{1,0:T(8,128)(2,1)S(1)}, u32[]{:S(2)}, u32[]{:S(2)}) collective-permute-start(bf16[256,1024]{1,0:T(8,128)(2,1)S(1)} %get-tuple-element.33), channel_id=1, source_target_pairs={{0,8},{4,12},{8,0},{12,4},{16,24},{20,28},{24,16},{28,20},{1,9},{5... | collective-permute-start | bytes 1572872 | tf_op jit(solution)/shard_map/ppermute | solution.py:22
  155.5 24.1 %collective-permute-start.27 = (bf16[256,1024]{1,0:T(8,128)(2,1)S(1)}, bf16[256,1024]{1,0:T(8,128)(2,1)S(1)}, u32[]{:S(2)}, u32[]{:S(2)}) collective-permute-start(bf16[256,1024]{1,0:T(8,128)(2,1)S(1)} %get-tuple-element.34), channel_id=1, source_target_pairs={{0,12},{4,8},{8,4},{12,0},{16,28},{20,24},{24,20},{28,16},{1,13},{... | collective-permute-start | bytes 1572872 | tf_op jit(solution)/shard_map/ppermute | solution.py:22
  158.9 27.3 %collective-permute-start.32 = (bf16[256,1024]{1,0:T(8,128)(2,1)S(1)}, bf16[256,1024]{1,0:T(8,128)(2,1)S(1)}, u32[]{:S(2)}, u32[]{:S(2)}) collective-permute-start(bf16[256,1024]{1,0:T(8,128)(2,1)S(1)} %get-tuple-element.36), channel_id=1, source_target_pairs={{0,4},{4,0},{8,12},{12,8},{16,20},{20,16},{24,28},{28,24},{1,5},{5... | collective-permute-start | bytes 1572872 | tf_op jit(solution)/shard_map/ppermute | solution.py:22
  160.5 30.3 %collective-permute-start.33 = (bf16[256,1024]{1,0:T(8,128)(2,1)S(1)}, bf16[256,1024]{1,0:T(8,128)(2,1)S(1)}, u32[]{:S(2)}, u32[]{:S(2)}) collective-permute-start(bf16[256,1024]{1,0:T(8,128)(2,1)S(1)} %get-tuple-element.37), channel_id=1, source_target_pairs={{0,8},{4,12},{8,0},{12,4},{16,24},{20,28},{24,16},{28,20},{1,9},{5... | collective-permute-start | bytes 1572872 | tf_op jit(solution)/shard_map/ppermute | solution.py:22
  164.9 36.8 %collective-permute-start.34 = (bf16[256,1024]{1,0:T(8,128)(2,1)S(1)}, bf16[256,1024]{1,0:T(8,128)(2,1)S(1)}, u32[]{:S(2)}, u32[]{:S(2)}) collective-permute-start(bf16[256,1024]{1,0:T(8,128)(2,1)S(1)} %get-tuple-element.38), channel_id=1, source_target_pairs={{0,12},{4,8},{8,4},{12,0},{16,28},{20,24},{24,20},{28,16},{1,13},{... | collective-permute-start | bytes 1572872 | tf_op jit(solution)/shard_map/ppermute | solution.py:22
